TPU v7x, 128 devices: a whole 4x4x4 slice. The times are simulated.
128 devices in a mesh: fs: 16 (over z, y), tp: 8 (over x, core).
Axes of the slice: x: 4, y: 4, z: 4, core: 2. Of those that a mesh axis runs over, the one named last changes fastest.
Arguments:
- weights_in: float32 [2, 2048, 5632], P(None, 'fs', 'tp'), may hold values from -6 to 6
- weights_mix: float32 [2048, 2048], P('fs', 'tp'), may hold values from -6 to 6
- momentum_in: float32 [2, 2048, 5632], P(None, 'fs', 'tp'), may hold values from -5 to 5
- momentum_mix: float32 [2048, 2048], P('fs', 'tp'), may hold values from -5 to 5
- grads_in: float32 [2, 2048, 5632], P(None, 'fs', 'tp'), may hold values from -5 to 5
- grads_mix: float32 [2048, 2048], P('fs', 'tp'), may hold values from -5 to 5
Outputs:
- momentum_in_next: float32 [2, 2048, 5632], P(None, 'fs', 'tp')
- momentum_mix_next: float32 [2048, 2048], P('fs', 'tp')
- weights_in_next: float32 [2, 2048, 5632], P(None, 'fs', 'tp')
- weights_mix_next: float32 [2048, 2048], P('fs', 'tp')
- update_in: float32 [2, 2048, 5632], P(None, 'fs', 'tp')
- update_mix: float32 [2048, 2048], P('fs', 'tp')
All inputs are finite; a program needn't handle non-finite values.
Results may differ from a plain program's by a relative error of at most 0.0003.
Values sent between devices are 32-bit elements; how exact they have to be, the bound alone decides.
No kernel may reach another device: no remote copies, remote signals or barrier semaphores. Data moves between devices by JAX's collectives and lax.ppermute only.
A program may use at most 128 MiB of HBM per device.

v0:
```python
import math
import jax
import jax.numpy as jnp
from jax import lax
from jax.sharding import PartitionSpec as P

D = 2048
FF = 5632
ITERS = 3
A_COEF = 3.4445
B_COEF = -4.775
C_COEF = 2.0315
MOMENTUM_DECAY = 0.95
STEP_RATE = 0.02
HIGH = lax.Precision.HIGHEST


def gather_turned(arrays, axis, dims):
    turned = [jnp.moveaxis(a, dim, 0) for a, dim in zip(arrays, dims)]
    both = jnp.concatenate([t.reshape(len(t), -1) for t in turned], axis=1)
    result, at, gathered = (lax.all_gather(both, axis, axis=0, tiled=True), 0, [])
    for t, dim in zip(turned, dims):
        share = result[:, at : at + t[0].size].reshape(-1, *t.shape[1:])
        gathered.append(jnp.moveaxis(share, 0, dim))
        at += t[0].size
    return tuple(gathered)


def rows_for(lines, peers):
    spare = -lines.shape[0] % peers
    if not spare:
        return lines
    return jnp.concatenate([lines, jnp.zeros((spare, *lines.shape[1:]), lines.dtype)])


def sum_by_parts(shard, axis):
    lines = shard.reshape(-1, *shard.shape[1:][-1:])
    own = lax.psum_scatter(
        rows_for(lines, lax.axis_size(axis)), axis, scatter_dimension=0, tiled=True
    )
    whole = lax.all_gather(own, axis).reshape(-1, *lines.shape[1:])
    return lax.slice_in_dim(whole, 0, len(lines)).reshape(shard.shape)


def scale_from(summed):
    return (0.5 * lax.rsqrt(jnp.maximum(summed / D, 1.0)))[:, None, None]


def block_trace(shard, row_start, col_start):
    row_ids = row_start + lax.iota(jnp.int32, shard.shape[1])[:, None]
    col_ids = col_start + lax.iota(jnp.int32, shard.shape[2])[None, :]
    return jnp.sum(jnp.where((row_ids == col_ids)[None], shard, 0.0), axis=(1, 2))


def local(weights_in, weights_mix, momentum_in, momentum_mix, grads_in, grads_mix):
    fs_pos = lax.axis_index("fs")
    tp_pos = lax.axis_index("tp")
    moment_in = MOMENTUM_DECAY * momentum_in + grads_in
    moment_mix = MOMENTUM_DECAY * momentum_mix + grads_mix
    local_in = moment_in
    local_mix = moment_mix[None]
    row_count = local_in.shape[1]
    block_width = local_mix.shape[2]
    for iteration in range(ITERS):
        cols_in, cols_mix = gather_turned((local_in, local_mix), "fs", (1, 1))
        partial_value = jnp.concatenate(
            [
                jnp.einsum("krc,ksc->krs", local_in, cols_in, precision=HIGH),
                jnp.einsum("krc,ksc->krs", local_mix, cols_mix, precision=HIGH),
            ]
        )
        gram_rows = sum_by_parts(partial_value, "tp")
        gram_block = lax.dynamic_slice_in_dim(gram_rows, tp_pos * block_width, block_width, 2)
        if iteration == 0:
            traces = block_trace(gram_block, fs_pos * row_count, tp_pos * block_width)
            scaling = scale_from(lax.psum(traces, ("fs", "tp")))
        factor = scaling if iteration == 0 else jnp.ones_like(scaling)
        gram_cols = lax.all_gather(gram_block, "fs", axis=1, tiled=True)
        square = jnp.einsum("krs,ksc->krc", gram_rows, gram_cols, precision=HIGH)
        poly_mat = factor**2 * B_COEF * gram_block + factor**4 * C_COEF * square
        poly_rows = lax.all_gather(poly_mat, "tp", axis=2, tiled=True)
        local_in = factor[:2] * (
            A_COEF * local_in + jnp.einsum("krs,ksc->krc", poly_rows[:2], cols_in, precision=HIGH)
        )
        local_mix = factor[2:] * (
            A_COEF * local_mix + jnp.einsum("krs,ksc->krc", poly_rows[2:], cols_mix, precision=HIGH)
        )
    step_in = local_in * math.sqrt(max(D, FF))
    step_mix = local_mix[0] * math.sqrt(D)
    return (
        moment_in,
        moment_mix,
        weights_in - STEP_RATE * step_in,
        weights_mix - STEP_RATE * step_mix,
        step_in,
        step_mix,
    )


def solution(mesh):
    in_specs = (
        P(None, "fs", "tp"),
        P("fs", "tp"),
        P(None, "fs", "tp"),
        P("fs", "tp"),
        P(None, "fs", "tp"),
        P("fs", "tp"),
    )
    out_specs = (
        P(None, "fs", "tp"),
        P("fs", "tp"),
        P(None, "fs", "tp"),
        P("fs", "tp"),
        P(None, "fs", "tp"),
        P("fs", "tp"),
    )
    return jax.shard_map(local, mesh=mesh, in_specs=in_specs, out_specs=out_specs, check_vma=False)
```

profile of v0, /device:TPU:1, one launch (start us, length us, event | category | flops | bytes accessed | tf_op | source)
XLA Modules:
  0.0 954.7 jit_solution(4597433947635089846)
XLA Ops:
  10.9 105.9 %all-gather.16.cloned.1.call-done = f32[2048,1664]{0,1:T(8,128)} async-done(((f32[128,1664]{0,1:T(8,128)}), f32[2048,1664]{0,1:T(8,128)}) %all-gather.16.cloned.1.call-update) | async-done | bytes 13631504 | tf_op jit(solution)/shard_map/all_gather | solution.py:21
  116.8 10.4 %slice.58 = f32[2048,1408]{0,1:T(8,128)} slice(f32[2048,1664]{0,1:T(8,128)} %all-gather.16.cloned.1.call-done), slice={[0:2048], [0:1408]} | slice | bytes 23068672 | tf_op jit(solution)/shard_map/slice | solution.py:23
  127.2 9.2 fusion.25
  141.2 33.7 %reduce-scatter.4.cloned.1.call-done = f32[48,2048]{1,0:T(8,128)} async-done(((f32[384,2048]{1,0:T(8,128)}), f32[48,2048]{1,0:T(8,128)}) %reduce-scatter.4.cloned.1.call-update) | async-done | bytes 393232 | tf_op jit(solution)/shard_map/reduce_scatter | solution.py:38
  175.1 31.3 %all-gather.34.cloned.1.call-done = f32[384,2048]{1,0:T(8,128)} async-done(((f32[48,2048]{1,0:T(8,128)}), f32[384,2048]{1,0:T(8,128)}) %all-gather.34.cloned.1.call-update) | async-done | bytes 3145744 | tf_op jit(solution)/shard_map/all_gather | solution.py:41
  208.3 67.5 %psum.7 = f32[3]{0:T(128)S(1)} all-reduce(f32[3]{0:T(128)S(1)} %get-tuple-element.8), channel_id=1, replica_groups=mesh['fs'=16,'tp'=8] {'fs','tp'}, use_global_device_ids=true, to_apply=%region_2.3 | all-reduce | flops 3 | bytes 24 | tf_op jit(solution)/shard_map/psum | solution.py:76
  284.9 23.8 %all-gather.20.cloned.1.call-done = f32[3,128,2048]{2,1,0:T(8,128)} async-done(((f32[3,128,256]{2,1,0:T(8,128)}), f32[3,128,2048]{2,1,0:T(8,128)}) %all-gather.20.cloned.1.call-update) | async-done | bytes 3145744 | tf_op jit(solution)/shard_map/all_gather | solution.py:81
  313.6 13.0 %fusion.9 = f32[2,128,704]{1,2,0:T(8,128)S(1)} fusion(f32[3,128,2048]{2,1,0:T(8,128)} %all-gather.20.cloned.1.call-done, f32[2,2048,704]{1,2,0:T(8,128)} %bitcast.65, f32[2,128,704]{1,2,0:T(8,128)S(1)} %multiply_add_fusion, f32[2]{0:T(128)S(1)} %bitcast.82), kind=kOutput, calls=%fused_computation.18 | convolution fusion | flops 4429725696 | bytes 16121864 | tf_op jit(solution)/shard_map/krs,ksc->krc/dot_general | solution.py:83
  327.9 102.1 %all-gather.22.cloned.1.call-done = f32[2048,1664]{0,1:T(8,128)} async-done(((f32[128,1664]{0,1:T(8,128)}), f32[2048,1664]{0,1:T(8,128)}) %all-gather.22.cloned.1.call-update) | async-done | bytes 13631504 | tf_op jit(solution)/shard_map/all_gather | solution.py:21
  429.9 10.4 %slice.61 = f32[2048,1408]{0,1:T(8,128)} slice(f32[2048,1664]{0,1:T(8,128)} %all-gather.22.cloned.1.call-done), slice={[0:2048], [0:1408]} | slice | bytes 23068672 | tf_op jit(solution)/shard_map/slice | solution.py:23
  440.3 9.2 fusion.26
  454.4 33.7 %reduce-scatter.6.cloned.1.call-done = f32[48,2048]{1,0:T(8,128)} async-done(((f32[384,2048]{1,0:T(8,128)}), f32[48,2048]{1,0:T(8,128)}) %reduce-scatter.6.cloned.1.call-update) | async-done | bytes 393232 | tf_op jit(solution)/shard_map/reduce_scatter | solution.py:38
  488.1 31.5 %all-gather.36.cloned.1.call-done = f32[384,2048]{1,0:T(8,128)} async-done(((f32[48,2048]{1,0:T(8,128)}), f32[384,2048]{1,0:T(8,128)}) %all-gather.36.cloned.1.call-update) | async-done | bytes 3145744 | tf_op jit(solution)/shard_map/all_gather | solution.py:41
  521.4 61.7 %all-gather.24.cloned.1.call-done = f32[3,2048,256]{2,1,0:T(8,128)} async-done(((f32[3,128,256]{2,1,0:T(8,128)}), f32[3,2048,256]{2,1,0:T(8,128)}) %all-gather.24.cloned.1.call-update) | async-done | bytes 6291472 | tf_op jit(solution)/shard_map/all_gather | solution.py:78
  591.8 27.5 %all-gather.26.cloned.1.call-done = f32[3,128,2048]{2,1,0:T(8,128)} async-done(((f32[3,128,256]{2,1,0:T(8,128)}), f32[3,128,2048]{2,1,0:T(8,128)}) %all-gather.26.cloned.1.call-update) | async-done | bytes 3145744 | tf_op jit(solution)/shard_map/all_gather | solution.py:81
  623.5 13.0 %convolution_add_fusion.1 = f32[2,128,704]{1,2,0:T(8,128)S(1)} fusion(f32[3,128,2048]{2,1,0:T(8,128)} %all-gather.26.cloned.1.call-done, f32[2,2048,704]{1,2,0:T(8,128)} %bitcast.69, f32[2,128,704]{1,2,0:T(8,128)S(1)} %fusion.9), kind=kOutput, calls=%fused_computation.16 | convolution fusion | flops 4429545472 | bytes 16121856 | tf_op jit(solution)/shard_map/krs,ksc->krc/dot_general | solution.py:83
  637.6 102.3 %all-gather.28.cloned.1.call-done = f32[2048,1664]{0,1:T(8,128)} async-done(((f32[128,1664]{0,1:T(8,128)}), f32[2048,1664]{0,1:T(8,128)}) %all-gather.28.cloned.1.call-update) | async-done | bytes 13631504 | tf_op jit(solution)/shard_map/all_gather | solution.py:21
  739.8 10.4 %slice.64 = f32[2048,1408]{0,1:T(8,128)} slice(f32[2048,1664]{0,1:T(8,128)} %all-gather.28.cloned.1.call-done), slice={[0:2048], [0:1408]} | slice | bytes 23068672 | tf_op jit(solution)/shard_map/slice | solution.py:23
  750.2 9.2 fusion.27
  764.2 33.7 %reduce-scatter.8.cloned.1.call-done = f32[48,2048]{1,0:T(8,128)} async-done(((f32[384,2048]{1,0:T(8,128)}), f32[48,2048]{1,0:T(8,128)}) %reduce-scatter.8.cloned.1.call-update) | async-done | bytes 393232 | tf_op jit(solution)/shard_map/reduce_scatter | solution.py:38
  798.0 31.5 %all-gather.38.cloned.1.call-done = f32[384,2048]{1,0:T(8,128)} async-done(((f32[48,2048]{1,0:T(8,128)}), f32[384,2048]{1,0:T(8,128)}) %all-gather.38.cloned.1.call-update) | async-done | bytes 3145744 | tf_op jit(solution)/shard_map/all_gather | solution.py:41
  831.5 61.4 %all-gather.30.cloned.1.call-done = f32[3,2048,256]{2,1,0:T(8,128)} async-done(((f32[3,128,256]{2,1,0:T(8,128)}), f32[3,2048,256]{2,1,0:T(8,128)}) %all-gather.30.cloned.1.call-update) | async-done | bytes 6291472 | tf_op jit(solution)/shard_map/all_gather | solution.py:78
  901.1 27.9 %all-gather.32.cloned.1.call-done = f32[3,128,2048]{2,1,0:T(8,128)} async-done(((f32[3,128,256]{2,1,0:T(8,128)}), f32[3,128,2048]{2,1,0:T(8,128)}) %all-gather.32.cloned.1.call-update) | async-done | bytes 3145744 | tf_op jit(solution)/shard_map/all_gather | solution.py:81
  934.0 13.9 %broadcast_multiply_fusion = (f32[2,128,704]{1,2,0:T(8,128)}, f32[2,128,704]{1,2,0:T(8,128)}) fusion(f32[2,128,704]{1,2,0:T(8,128)S(1)} %copy-done.3, f32[3,128,2048]{2,1,0:T(8,128)S(1)} %copy-done.1, f32[2,2048,704]{1,2,0:T(8,128)} %bitcast.67, f32[2,128,704]{1,2,0:T(8,128)S(1)} %convolution_add_fusion.1), kind=kOutput, calls=%fused_computation.38 | convolution fusion | flops 4430086144 | bytes 17563648 | tf_op jit(solution)/shard_map/krs,ksc->krc/dot_general | solution.py:83
  (70 shorter events, 66.3 us)
Async XLA Ops:
  7.2 109.6 %all-gather.16.cloned.1.call-start = ((), (), s32[]{:S(2)}) async-start(), calls=%async_computation.3 | async-start | bytes 14483456 | tf_op jit(solution)/shard_map/all_gather | solution.py:21
  8.2 300.5 %copy-start.2 = (f32[128,256]{1,0:T(8,128)}, f32[128,256]{1,0:T(8,128)S(1)}, u32[]{:S(2)}) copy-start(f32[128,256]{1,0:T(8,128)S(1)} %multiply_add_fusion.1) | copy-start | bytes 393220
  9.7 303.9 %copy-start = (f32[2,128,704]{1,2,0:T(8,128)}, f32[2,128,704]{1,2,0:T(8,128)S(1)}, u32[]{:S(2)}) copy-start(f32[2,128,704]{1,2,0:T(8,128)S(1)} %multiply_add_fusion) | copy-start | bytes 2162692
  10.8 164.1 %reduce-scatter.4.cloned.1.call-start = ((), (), s32[]{:S(2)}) async-start(), calls=%async_computation.4 | async-start | bytes 3538944 | tf_op jit(solution)/shard_map/reduce_scatter | solution.py:38
  141.2 65.3 %all-gather.34.cloned.1.call-start = ((), (), s32[]{:S(2)}) async-start(), calls=%async_computation.15 | async-start | bytes 3538944 | tf_op jit(solution)/shard_map/all_gather | solution.py:41
  174.9 100.9 %all-gather.18.cloned.1.call-start = ((), (), s32[]{:S(2)}) async-start(), calls=%async_computation.5 | async-start | bytes 6684672 | tf_op jit(solution)/shard_map/all_gather | solution.py:78
  208.2 100.5 %all-gather.20.cloned.1.call-start = ((), (), s32[]{:S(2)}) async-start(), calls=%async_computation.6 | async-start | bytes 3538944 | tf_op jit(solution)/shard_map/all_gather | solution.py:81
  284.1 145.9 %all-gather.22.cloned.1.call-start = ((), (), s32[]{:S(2)}) async-start(), calls=%async_computation.7 | async-start | bytes 14483456 | tf_op jit(solution)/shard_map/all_gather | solution.py:21
  327.6 160.4 %reduce-scatter.6.cloned.1.call-start = ((), (), s32[]{:S(2)}) async-start(), calls=%async_computation.8 | async-start | bytes 3538944 | tf_op jit(solution)/shard_map/reduce_scatter | solution.py:38
  454.3 65.3 %all-gather.36.cloned.1.call-start = ((), (), s32[]{:S(2)}) async-start(), calls=%async_computation.16 | async-start | bytes 3538944 | tf_op jit(solution)/shard_map/all_gather | solution.py:41
  488.1 95.1 %all-gather.24.cloned.1.call-start = ((), (), s32[]{:S(2)}) async-start(), calls=%async_computation.9 | async-start | bytes 6684672 | tf_op jit(solution)/shard_map/all_gather | solution.py:78
  521.4 97.9 %all-gather.26.cloned.1.call-start = ((), (), s32[]{:S(2)}) async-start(), calls=%async_computation.10 | async-start | bytes 3538944 | tf_op jit(solution)/shard_map/all_gather | solution.py:81
  591.3 148.5 %all-gather.28.cloned.1.call-start = ((), (), s32[]{:S(2)}) async-start(), calls=%async_computation.11 | async-start | bytes 14483456 | tf_op jit(solution)/shard_map/all_gather | solution.py:21
  637.5 160.4 %reduce-scatter.8.cloned.1.call-start = ((), (), s32[]{:S(2)}) async-start(), calls=%async_computation.12 | async-start | bytes 3538944 | tf_op jit(solution)/shard_map/reduce_scatter | solution.py:38
  764.2 65.3 %all-gather.38.cloned.1.call-start = ((), (), s32[]{:S(2)}) async-start(), calls=%async_computation.17 | async-start | bytes 3538944 | tf_op jit(solution)/shard_map/all_gather | solution.py:41
  797.9 94.9 %all-gather.30.cloned.1.call-start = ((), (), s32[]{:S(2)}) async-start(), calls=%async_computation.13 | async-start | bytes 6684672 | tf_op jit(solution)/shard_map/all_gather | solution.py:78
  831.2 97.8 %copy-start.4 = (f32[128,256]{1,0:T(8,128)S(1)}, f32[128,256]{1,0:T(8,128)}, u32[]{:S(2)}) copy-start(f32[128,256]{1,0:T(8,128)} %param.7) | copy-start | bytes 393220
  831.3 97.8 %all-gather.32.cloned.1.call-start = ((), (), s32[]{:S(2)}) async-start(), calls=%async_computation.14 | async-start | bytes 3538944 | tf_op jit(solution)/shard_map/all_gather | solution.py:81
  901.1 33.0 %copy-start.3 = (f32[2,128,704]{1,2,0:T(8,128)S(1)}, f32[2,128,704]{1,2,0:T(8,128)}, u32[]{:S(2)}) copy-start(f32[2,128,704]{1,2,0:T(8,128)} %param.6) | copy-start | bytes 2162692
  929.0 5.0 copy-start.1
Sparse Core Ops, SparseCore 0:
  10.9 105.7 all-gather.15
  141.3 33.5 reduce-scatter.3
  176.6 29.8 all-gather.33
  209.0 61.3 all-gather.17
  284.2 24.4 all-gather.19
  327.7 102.1 all-gather.21
  454.4 33.5 reduce-scatter.5
  489.7 29.8 all-gather.35
  522.3 60.7 all-gather.23
  591.5 27.7 all-gather.25
  637.6 102.1 all-gather.27
  764.3 33.5 reduce-scatter.7
  799.6 29.8 all-gather.37
  832.0 60.7 all-gather.29
  901.2 27.7 all-gather.31
where the time goes:
time: 963 us; the launch traced here: 955 us
  waiting for transfers between devices  708 us (74%)
  matrix products  114 us (12%)
  blocking collectives  67.5 us (7%)
  local copies, waits for them, and re-layouts  35.7 us (4%)
  between operations  14.3 us (1%)
  other arithmetic  13.1 us (1%)
    all_gather x3, waiting for transfers between devices, gather_turned(): lax.all_gather(both, axis, axis=0, tiled=True)  310 us
    all_gather x3, waiting for transfers between devices, local(): gram_cols = lax.all_gather(gram_block, 'fs', axis=1, tiled=True)  123 us
    reduce_scatter x3, waiting for transfers between devices, sum_by_parts(): lax.psum_scatter(rows_for(lines, lax.axis_size(axis)), axis, scatter_dime...  101 us
    all_gather x3, waiting for transfers between devices, sum_by_parts(): whole = lax.all_gather(own, axis).reshape(-1, *lines.shape[1:])  94.3 us
    all_gather x3, waiting for transfers between devices, local(): poly_rows = lax.all_gather(poly_mat, 'tp', axis=2, tiled=True)  79.3 us
    psum x1, blocking collectives, local(): scaling = scale_from(lax.psum(traces, ('fs', 'tp')))  67.5 us
    dot_general x3, matrix products, local(): jnp.einsum('krs,ksc->krc', poly_rows[:2], cols_in, precision=HIGH)  39.9 us
    slice x3, local copies, waits for them, and re-layouts, gather_turned(): share = result[:, at:at + t[0].size].reshape(-1, *t.shape[1:])  31.2 us
  transfers between devices with their start and end apart: 15, of which 14 were waited for; matrix products, arithmetic and copies ran while one was open for 0% of the time, Pallas kernels for 0%

commit v1 on v0

--- a/solution.py
+++ b/solution.py
@@ -78,7 +78,7 @@
         gram_cols = lax.all_gather(gram_block, "fs", axis=1, tiled=True)
         square = jnp.einsum("krs,ksc->krc", gram_rows, gram_cols, precision=HIGH)
         poly_mat = factor**2 * B_COEF * gram_block + factor**4 * C_COEF * square
-        poly_rows = lax.all_gather(poly_mat, "tp", axis=2, tiled=True)
+        poly_rows = jnp.concatenate(lax.all_gather(poly_mat, "tp"), axis=2)
         local_in = factor[:2] * (
             A_COEF * local_in + jnp.einsum("krs,ksc->krc", poly_rows[:2], cols_in, precision=HIGH)
         )

time: 963 us -> 975 us (1.012)
  local copies, waits for them, and re-layouts: 35.7 us -> 51.1 us
    slice x0 -> x9, local copies, waits for them, and re-layouts: none -> 10.2 us  [the longest x6 8.15 us: local(): poly_rows[2:]]
where the time goes in v1:
time: 975 us; the launch traced here: 966 us
  waiting for transfers between devices  708 us (73%)
  matrix products  110 us (11%)
  blocking collectives  67.5 us (7%)
  local copies, waits for them, and re-layouts  51.1 us (5%)
  between operations  14.6 us (1%)
  other arithmetic  13.1 us (1%)
    all_gather x3, waiting for transfers between devices, gather_turned(): lax.all_gather(both, axis, axis=0, tiled=True)  310 us
    all_gather x3, waiting for transfers between devices, local(): gram_cols = lax.all_gather(gram_block, 'fs', axis=1, tiled=True)  123 us
    reduce_scatter x3, waiting for transfers between devices, sum_by_parts(): lax.psum_scatter(rows_for(lines, lax.axis_size(axis)), axis, scatter_dime...  101 us
    all_gather x3, waiting for transfers between devices, sum_by_parts(): whole = lax.all_gather(own, axis).reshape(-1, *lines.shape[1:])  94.3 us
    all_gather x3, waiting for transfers between devices, local(): poly_rows = jnp.concatenate(lax.all_gather(poly_mat, 'tp'), axis=2)  79.5 us
    psum x1, blocking collectives, local(): scaling = scale_from(lax.psum(traces, ('fs', 'tp')))  67.5 us
    dot_general x3, matrix products, local(): jnp.einsum('krs,ksc->krc', poly_rows[:2], cols_in, precision=HIGH)  37.7 us
    slice x3, local copies, waits for them, and re-layouts, gather_turned(): share = result[:, at:at + t[0].size].reshape(-1, *t.shape[1:])  31.3 us
  transfers between devices with their start and end apart: 15, of which 14 were waited for; matrix products, arithmetic and copies ran while one was open for 0% of the time, Pallas kernels for 0%

profile of v1, /device:TPU:1, one launch (start us, length us, event | category | flops | bytes accessed | tf_op | source)
XLA Modules:
  0.0 965.9 jit_solution(4677038367554011040)
XLA Ops:
  10.9 105.9 %all-gather.19.cloned.1.call-done = f32[2048,1664]{0,1:T(8,128)} async-done(((f32[128,1664]{0,1:T(8,128)}), f32[2048,1664]{0,1:T(8,128)}) %all-gather.19.cloned.1.call-update) | async-done | bytes 13631504 | tf_op jit(solution)/shard_map/all_gather | solution.py:21
  116.8 10.4 %slice.73 = f32[2048,1408]{0,1:T(8,128)} slice(f32[2048,1664]{0,1:T(8,128)} %all-gather.19.cloned.1.call-done), slice={[0:2048], [0:1408]} | slice | bytes 23068672 | tf_op jit(solution)/shard_map/slice | solution.py:23
  127.2 9.2 fusion.25
  141.2 33.7 %reduce-scatter.4.cloned.1.call-done = f32[48,2048]{1,0:T(8,128)} async-done(((f32[384,2048]{1,0:T(8,128)}), f32[48,2048]{1,0:T(8,128)}) %reduce-scatter.4.cloned.1.call-update) | async-done | bytes 393232 | tf_op jit(solution)/shard_map/reduce_scatter | solution.py:38
  175.1 31.3 %all-gather.31.cloned.1.call-done = f32[384,2048]{1,0:T(8,128)} async-done(((f32[48,2048]{1,0:T(8,128)}), f32[384,2048]{1,0:T(8,128)}) %all-gather.31.cloned.1.call-update) | async-done | bytes 3145744 | tf_op jit(solution)/shard_map/all_gather | solution.py:41
  208.3 67.5 %psum.7 = f32[3]{0:T(128)S(1)} all-reduce(f32[3]{0:T(128)S(1)} %get-tuple-element.8), channel_id=1, replica_groups=mesh['fs'=16,'tp'=8] {'fs','tp'}, use_global_device_ids=true, to_apply=%region_2.3 | all-reduce | flops 3 | bytes 24 | tf_op jit(solution)/shard_map/psum | solution.py:76
  284.9 23.8 %all-gather.33.cloned.1.call-done = f32[24,128,256]{2,1,0:T(8,128)} async-done(((f32[3,128,256]{2,1,0:T(8,128)}), f32[24,128,256]{2,1,0:T(8,128)}) %all-gather.33.cloned.1.call-update) | async-done | bytes 3145744 | tf_op jit(solution)/shard_map/all_gather | solution.py:81
  317.9 12.5 %fusion.9 = f32[2,128,704]{1,2,0:T(8,128)S(1)} fusion(f32[2,128,2048]{2,1,0:T(8,128)} %bitcast.90, f32[2,2048,704]{1,2,0:T(8,128)} %bitcast.78, f32[2,128,704]{1,2,0:T(8,128)S(1)} %multiply_add_fusion, f32[2]{0:T(128)S(1)} %bitcast.107), kind=kOutput, calls=%fused_computation.21 | convolution fusion | flops 4429725696 | bytes 15073288 | tf_op jit(solution)/shard_map/krs,ksc->krc/dot_general | solution.py:83
  331.8 101.8 %all-gather.23.cloned.1.call-done = f32[2048,1664]{0,1:T(8,128)} async-done(((f32[128,1664]{0,1:T(8,128)}), f32[2048,1664]{0,1:T(8,128)}) %all-gather.23.cloned.1.call-update) | async-done | bytes 13631504 | tf_op jit(solution)/shard_map/all_gather | solution.py:21
  433.7 10.4 %slice.77 = f32[2048,1408]{0,1:T(8,128)} slice(f32[2048,1664]{0,1:T(8,128)} %all-gather.23.cloned.1.call-done), slice={[0:2048], [0:1408]} | slice | bytes 23068672 | tf_op jit(solution)/shard_map/slice | solution.py:23
  444.1 9.2 fusion.26
  458.1 33.6 %reduce-scatter.6.cloned.1.call-done = f32[48,2048]{1,0:T(8,128)} async-done(((f32[384,2048]{1,0:T(8,128)}), f32[48,2048]{1,0:T(8,128)}) %reduce-scatter.6.cloned.1.call-update) | async-done | bytes 393232 | tf_op jit(solution)/shard_map/reduce_scatter | solution.py:38
  491.8 31.5 %all-gather.35.cloned.1.call-done = f32[384,2048]{1,0:T(8,128)} async-done(((f32[48,2048]{1,0:T(8,128)}), f32[384,2048]{1,0:T(8,128)}) %all-gather.35.cloned.1.call-update) | async-done | bytes 3145744 | tf_op jit(solution)/shard_map/all_gather | solution.py:41
  525.2 61.7 %all-gather.25.cloned.1.call-done = f32[3,2048,256]{2,1,0:T(8,128)} async-done(((f32[3,128,256]{2,1,0:T(8,128)}), f32[3,2048,256]{2,1,0:T(8,128)}) %all-gather.25.cloned.1.call-update) | async-done | bytes 6291472 | tf_op jit(solution)/shard_map/all_gather | solution.py:78
  595.3 27.7 %all-gather.37.cloned.1.call-done = f32[24,128,256]{2,1,0:T(8,128)} async-done(((f32[3,128,256]{2,1,0:T(8,128)}), f32[24,128,256]{2,1,0:T(8,128)}) %all-gather.37.cloned.1.call-update) | async-done | bytes 3145744 | tf_op jit(solution)/shard_map/all_gather | solution.py:81
  626.4 12.1 %convolution_add_fusion.1 = f32[2,128,704]{1,2,0:T(8,128)S(1)} fusion(f32[2,128,2048]{2,1,0:T(8,128)S(1)} %bitcast.89, f32[2,2048,704]{1,2,0:T(8,128)} %bitcast.82, f32[2,128,704]{1,2,0:T(8,128)S(1)} %fusion.9), kind=kOutput, calls=%fused_computation.19 | convolution fusion | flops 4429545472 | bytes 15073280 | tf_op jit(solution)/shard_map/krs,ksc->krc/dot_general | solution.py:83
  643.4 102.3 %all-gather.27.cloned.1.call-done = f32[2048,1664]{0,1:T(8,128)} async-done(((f32[128,1664]{0,1:T(8,128)}), f32[2048,1664]{0,1:T(8,128)}) %all-gather.27.cloned.1.call-update) | async-done | bytes 13631504 | tf_op jit(solution)/shard_map/all_gather | solution.py:21
  745.7 10.4 %slice.81 = f32[2048,1408]{0,1:T(8,128)} slice(f32[2048,1664]{0,1:T(8,128)} %all-gather.27.cloned.1.call-done), slice={[0:2048], [0:1408]} | slice | bytes 23068672 | tf_op jit(solution)/shard_map/slice | solution.py:23
  756.1 9.2 fusion.27
  770.1 33.7 %reduce-scatter.8.cloned.1.call-done = f32[48,2048]{1,0:T(8,128)} async-done(((f32[384,2048]{1,0:T(8,128)}), f32[48,2048]{1,0:T(8,128)}) %reduce-scatter.8.cloned.1.call-update) | async-done | bytes 393232 | tf_op jit(solution)/shard_map/reduce_scatter | solution.py:38
  803.9 31.5 %all-gather.39.cloned.1.call-done = f32[384,2048]{1,0:T(8,128)} async-done(((f32[48,2048]{1,0:T(8,128)}), f32[384,2048]{1,0:T(8,128)}) %all-gather.39.cloned.1.call-update) | async-done | bytes 3145744 | tf_op jit(solution)/shard_map/all_gather | solution.py:41
  837.4 61.3 %all-gather.29.cloned.1.call-done = f32[3,2048,256]{2,1,0:T(8,128)} async-done(((f32[3,128,256]{2,1,0:T(8,128)}), f32[3,2048,256]{2,1,0:T(8,128)}) %all-gather.29.cloned.1.call-update) | async-done | bytes 6291472 | tf_op jit(solution)/shard_map/all_gather | solution.py:78
  906.9 27.9 %all-gather.41.cloned.1.call-done = f32[24,128,256]{2,1,0:T(8,128)} async-done(((f32[3,128,256]{2,1,0:T(8,128)}), f32[24,128,256]{2,1,0:T(8,128)}) %all-gather.41.cloned.1.call-update) | async-done | bytes 3145744 | tf_op jit(solution)/shard_map/all_gather | solution.py:81
  941.7 13.1 %broadcast_multiply_fusion = (f32[2,128,704]{1,2,0:T(8,128)}, f32[2,128,704]{1,2,0:T(8,128)}) fusion(f32[2,128,704]{1,2,0:T(8,128)S(1)} %copy-done.6, f32[2,128,2048]{2,1,0:T(8,128)S(1)} %bitcast.91, f32[2,2048,704]{1,2,0:T(8,128)} %bitcast.80, f32[2,128,704]{1,2,0:T(8,128)S(1)} %convolution_add_fusion.1), kind=kOutput, calls=%fused_computation.38 | convolution fusion | flops 4430086144 | bytes 16515072 | tf_op jit(solution)/shard_map/krs,ksc->krc/dot_general | solution.py:83
  (88 shorter events, 79.6 us)
Async XLA Ops:
  7.2 109.6 %all-gather.19.cloned.1.call-start = ((), (), s32[]{:S(2)}) async-start(), calls=%async_computation.3 | async-start | bytes 14483456 | tf_op jit(solution)/shard_map/all_gather | solution.py:21
  8.2 305.5 %copy-start.2 = (f32[128,256]{1,0:T(8,128)}, f32[128,256]{1,0:T(8,128)S(1)}, u32[]{:S(2)}) copy-start(f32[128,256]{1,0:T(8,128)S(1)} %multiply_add_fusion.1) | copy-start | bytes 393220
  9.7 308.2 %copy-start = (f32[2,128,704]{1,2,0:T(8,128)}, f32[2,128,704]{1,2,0:T(8,128)S(1)}, u32[]{:S(2)}) copy-start(f32[2,128,704]{1,2,0:T(8,128)S(1)} %multiply_add_fusion) | copy-start | bytes 2162692
  10.8 164.1 %reduce-scatter.4.cloned.1.call-start = ((), (), s32[]{:S(2)}) async-start(), calls=%async_computation.4 | async-start | bytes 3538944 | tf_op jit(solution)/shard_map/reduce_scatter | solution.py:38
  141.2 65.3 %all-gather.31.cloned.1.call-start = ((), (), s32[]{:S(2)}) async-start(), calls=%async_computation.12 | async-start | bytes 3538944 | tf_op jit(solution)/shard_map/all_gather | solution.py:41
  174.9 100.9 %all-gather.21.cloned.1.call-start = ((), (), s32[]{:S(2)}) async-start(), calls=%async_computation.5 | async-start | bytes 6684672 | tf_op jit(solution)/shard_map/all_gather | solution.py:78
  208.2 100.5 %all-gather.33.cloned.1.call-start = ((), (), s32[]{:S(2)}) async-start(), calls=%async_computation.13 | async-start | bytes 3538944 | tf_op jit(solution)/shard_map/all_gather | solution.py:81
  284.1 149.6 %all-gather.23.cloned.1.call-start = ((), (), s32[]{:S(2)}) async-start(), calls=%async_computation.6 | async-start | bytes 14483456 | tf_op jit(solution)/shard_map/all_gather | solution.py:21
  317.8 135.5 %copy-start.3 = (f32[128,256]{1,0:T(8,128)}, f32[128,256]{1,0:T(8,128)S(1)}, u32[]{:S(2)}) copy-start(f32[128,256]{1,0:T(8,128)S(1)} %fusion.16) | copy-start | bytes 393220
  331.4 160.4 %reduce-scatter.6.cloned.1.call-start = ((), (), s32[]{:S(2)}) async-start(), calls=%async_computation.7 | async-start | bytes 3538944 | tf_op jit(solution)/shard_map/reduce_scatter | solution.py:38
  458.1 65.3 %all-gather.35.cloned.1.call-start = ((), (), s32[]{:S(2)}) async-start(), calls=%async_computation.14 | async-start | bytes 3538944 | tf_op jit(solution)/shard_map/all_gather | solution.py:41
  491.8 95.1 %all-gather.25.cloned.1.call-start = ((), (), s32[]{:S(2)}) async-start(), calls=%async_computation.8 | async-start | bytes 6684672 | tf_op jit(solution)/shard_map/all_gather | solution.py:78
  525.1 97.9 %all-gather.37.cloned.1.call-start = ((), (), s32[]{:S(2)}) async-start(), calls=%async_computation.15 | async-start | bytes 3538944 | tf_op jit(solution)/shard_map/all_gather | solution.py:81
  595.1 150.6 %all-gather.27.cloned.1.call-start = ((), (), s32[]{:S(2)}) async-start(), calls=%async_computation.9 | async-start | bytes 14483456 | tf_op jit(solution)/shard_map/all_gather | solution.py:21
  642.3 123.0 %copy-start.4 = (f32[128,256]{1,0:T(8,128)}, f32[128,256]{1,0:T(8,128)S(1)}, u32[]{:S(2)}) copy-start(f32[128,256]{1,0:T(8,128)S(1)} %fusion.19) | copy-start | bytes 393220
  643.4 160.4 %reduce-scatter.8.cloned.1.call-start = ((), (), s32[]{:S(2)}) async-start(), calls=%async_computation.10 | async-start | bytes 3538944 | tf_op jit(solution)/shard_map/reduce_scatter | solution.py:38
  770.1 65.3 %all-gather.39.cloned.1.call-start = ((), (), s32[]{:S(2)}) async-start(), calls=%async_computation.16 | async-start | bytes 3538944 | tf_op jit(solution)/shard_map/all_gather | solution.py:41
  803.8 94.9 %all-gather.29.cloned.1.call-start = ((), (), s32[]{:S(2)}) async-start(), calls=%async_computation.11 | async-start | bytes 6684672 | tf_op jit(solution)/shard_map/all_gather | solution.py:78
  837.1 97.8 %all-gather.41.cloned.1.call-start = ((), (), s32[]{:S(2)}) async-start(), calls=%async_computation.17 | async-start | bytes 3538944 | tf_op jit(solution)/shard_map/all_gather | solution.py:81
  938.9 2.8 copy-start.6
  941.7 13.1 %copy-start.1 = (f32[1,128,8,256]{1,3,2,0:T(8,128)S(1)}, f32[1,128,8,256]{1,3,2,0:T(8,128)}, u32[]{:S(2)}) copy-start(f32[1,128,8,256]{1,3,2,0:T(8,128)} %copy.41) | copy-start | bytes 3145732
  941.7 13.1 %copy-start.5 = (f32[128,256]{1,0:T(8,128)S(1)}, f32[128,256]{1,0:T(8,128)}, u32[]{:S(2)}) copy-start(f32[128,256]{1,0:T(8,128)} %copy-done.4) | copy-start | bytes 393220
  941.7 13.1 %copy-start.7 = (f32[128,256]{1,0:T(8,128)S(1)}, f32[128,256]{1,0:T(8,128)}, u32[]{:S(2)}) copy-start(f32[128,256]{1,0:T(8,128)} %param.7) | copy-start | bytes 393220
Sparse Core Ops, SparseCore 0:
  11.0 105.7 all-gather.18
  141.3 33.5 reduce-scatter.3
  176.6 29.8 all-gather.30
  209.0 61.4 all-gather.20
  284.2 24.4 all-gather.32
  331.5 102.1 all-gather.22
  458.2 33.5 reduce-scatter.5
  493.4 29.8 all-gather.34
  526.1 60.7 all-gather.24
  595.2 27.7 all-gather.36
  643.5 102.1 all-gather.26
  770.2 33.5 reduce-scatter.7
  805.5 29.8 all-gather.38
  837.9 60.7 all-gather.28
  907.1 27.7 all-gather.40
